TPU v7x, 32 devices: a whole 2x2x4 slice. The times are simulated.
32 devices in a mesh: gr: 2 (over x), fs: 8 (over z, y), tp: 2 (over core).
Axes of the slice: x: 2, y: 2, z: 4, core: 2. Of those that a mesh axis runs over, the one named last changes fastest.
Arguments:
- tokens: bfloat16 [4096, 2048], P(('gr', 'tp'), 'fs'), may hold values from -400 to 400
- norm_gain: float32 [2048], P('fs'), may hold values from 0.1 to 1.9
- up_weight: float32 [2048, 8192], P('fs', ('gr', 'tp')), may hold values from -0.125 to 0.125
- down_weight: float32 [8192, 2048], P('fs', ('gr', 'tp')), may hold values from -0.09375 to 0.09375
Outputs:
- mixed: bfloat16 [2048, 4096], P('fs', ('gr', 'tp'))
- up_ready: bfloat16 [2048, 8192], P(None, 'fs')
- down_ready: bfloat16 [8192, 2048], P('fs')
All inputs are finite; a program needn't handle non-finite values.
Results may differ from a plain program's by a relative error of at most 0.023.
Values may be sent and summed in bfloat16 or wider, within the bound.
No kernel may reach another device: no remote copies, remote signals or barrier semaphores. Data moves between devices by JAX's collectives and lax.ppermute only.
A program may use at most 64 MiB of HBM per device.

v0:
```python
import jax
import jax.numpy as jnp
from jax import lax
from jax.sharding import PartitionSpec as P

epsilon = 1e-06


def shards(tokens, norm_gain, up_weight, down_weight):
    folded = (norm_gain[:, None] * up_weight).astype(jnp.bfloat16)
    down_cast = down_weight.astype(jnp.bfloat16)
    fs_count = lax.axis_size("fs")
    group_count = lax.axis_size(("gr", "tp"))
    rows_here, cols_here = folded.shape
    sub_rows = rows_here // group_count
    row_groups = folded.reshape(group_count, sub_rows, cols_here)
    full_rows = lax.all_to_all(row_groups, ("gr", "tp"), split_axis=0, concat_axis=2, tiled=True)
    full_width = full_rows.shape[2]
    unit_width = full_width // fs_count
    by_unit = full_rows.reshape(1, sub_rows, fs_count, unit_width)
    by_owner = lax.all_to_all(by_unit, "fs", split_axis=2, concat_axis=0, tiled=True)
    arranged = by_owner.reshape(fs_count, 1, sub_rows, unit_width)
    stacked, down_full = (
        lax.all_gather(arranged, ("gr", "tp"), axis=1, tiled=True),
        lax.all_gather(down_cast, ("gr", "tp"), axis=1, tiled=True),
    )
    up_full = stacked.reshape(fs_count * group_count * sub_rows, unit_width)
    model_width = up_full.shape[0]
    piece = lax.all_gather(tokens, "fs", axis=1, tiled=True)
    running = jnp.dot(piece, up_full, preferred_element_type=jnp.float32)
    piece_wide = piece.astype(jnp.float32)
    squares = jnp.sum(piece_wide * piece_wide, axis=1)
    raw_up, squares = (running, squares)
    row_scale = lax.rsqrt(squares / model_width + epsilon)
    hidden = jnp.square(jax.nn.relu(raw_up * row_scale[:, None])).astype(jnp.bfloat16)
    outcome = lax.psum_scatter(
        lax.dot_general(
            down_full, hidden, (((0,), (1,)), ((), ())), preferred_element_type=jnp.float32
        ).astype(jnp.bfloat16),
        "fs",
        scatter_dimension=0,
        tiled=True,
    )
    return (outcome, up_full, down_full)


def solution(mesh):
    in_specs = (P(("gr", "tp"), "fs"), P("fs"), P("fs", ("gr", "tp")), P("fs", ("gr", "tp")))
    out_specs = (P("fs", ("gr", "tp")), P(None, "fs"), P("fs", None))
    return jax.shard_map(shards, mesh=mesh, in_specs=in_specs, out_specs=out_specs, check_vma=False)
```

profile of v0, /device:TPU:0, one launch (start us, length us, event | category | flops | bytes accessed | tf_op | source)
XLA Modules:
  0.0 292.2 jit_solution(18041260175511250311)
XLA Ops:
  7.2 0.0 all-gather.5.cloned.1.call-start
  7.2 0.7 all-gather.5.cloned.1.call-update
  7.9 0.0 all-gather.9.cloned.1.call-start
  7.9 1.8 multiply_convert_fusion.1
  9.7 18.5 %all_to_all.30 = bf16[4,64,2048]{2,1,0:T(8,128)(2,1)S(1)} all-to-all(bf16[4,64,2048]{2,1,0:T(8,128)(2,1)S(1)} %bitcast.19), channel_id=1, replica_groups=mesh['gr'=2,'fs'=8,'tp'=2] {'gr','tp'}, dimensions={0} | all-to-all | bytes 2097152 | tf_op jit(solution)/shard_map/all_to_all | solution.py:17
  28.2 0.8 copy.13
  29.0 0.3 reshape.27
  29.3 0.6 copy.14
  29.9 0.0 copy-start
  29.9 53.7 %all_to_all.31 = bf16[1,64,8,1024]{3,1,0,2:T(8,128)(2,1)} all-to-all(bf16[1,64,8,1024]{3,1,0,2:T(8,128)(2,1)S(1)} %copy.14), channel_id=1, replica_groups=mesh['gr'=2,'fs'=8,'tp'=2] {'fs'}, dimensions={2} | all-to-all | bytes 2097152 | tf_op jit(solution)/shard_map/all_to_all | solution.py:21
  83.6 0.0 all-gather.9.cloned.1.call-update
  83.6 0.0 all-gather.7.cloned.1.call-start
  83.7 0.0 copy-done
  83.7 1.1 convert_element_type.22
  84.8 0.0 all-gather.7.cloned.1.call-update
  84.8 0.0 reduce-scatter.2.cloned.1.call-start
  84.9 18.0 %all-gather.5.cloned.1.call-done = bf16[1024,2048]{1,0:T(8,128)(2,1)} async-done(((bf16[1024,256]{1,0:T(8,128)(2,1)}), bf16[1024,2048]{1,0:T(8,128)(2,1)}) %all-gather.5.cloned.1.call-update) | async-done | bytes 4194320 | tf_op jit(solution)/shard_map/all_gather | solution.py:29
  102.8 3.1 %multiply_reduce_fusion = f32[1024]{0:T(1024)S(1)} fusion(bf16[1024,2048]{1,0:T(8,128)(2,1)} %all-gather.5.cloned.1.call-done), kind=kLoop, calls=%fused_computation | loop fusion | flops 6290432 | bytes 4198400 | tf_op jit(solution)/shard_map/reduce_sum | solution.py:32
  105.9 32.9 %all-gather.9.cloned.1.call-done = bf16[8,4,64,1,1024]{4,2,3,0,1:T(8,128)(2,1)} async-done(((bf16[8,1,64,1,1024]{4,2,3,0,1:T(8,128)(2,1)}), bf16[8,4,64,1,1024]{4,2,3,0,1:T(8,128)(2,1)}) %all-gather.9.cloned.1.call-update) | async-done | bytes 4194320 | tf_op jit(solution)/shard_map/all_gather | solution.py:24
  138.8 4.9 %copy.16 = bf16[8,4,64,1,1024]{4,2,1,0,3:T(8,128)(2,1)} copy(bf16[8,4,64,1,1024]{4,2,3,0,1:T(8,128)(2,1)} %all-gather.9.cloned.1.call-done) | data formatting | bytes 8388608 | tf_op jit(solution)/shard_map/all_gather | solution.py:24
  143.7 31.7 %all-gather.7.cloned.1.call-done = bf16[1024,2048]{1,0:T(8,128)(2,1)} async-done(((bf16[1024,512]{1,0:T(8,128)(2,1)}), bf16[1024,2048]{1,0:T(8,128)(2,1)}) %all-gather.7.cloned.1.call-update) | async-done | bytes 4194320 | tf_op jit(solution)/shard_map/all_gather | solution.py:25
  175.5 14.5 %convert_bitcast_fusion = bf16[2048,1024]{0,1:T(8,128)(2,1)} fusion(bf16[1024,2048]{1,0:T(8,128)(2,1)} %all-gather.7.cloned.1.call-done, bf16[2048,1024]{1,0:T(8,128)(2,1)} %bitcast.15, bf16[1024,2048]{1,0:T(8,128)(2,1)} %all-gather.5.cloned.1.call-done, f32[1024]{0:T(1024)S(1)} %add_rsqrt_fusion), kind=kOutput, calls=%fused_computation.1 | convolution fusion | flops 8596226048 | bytes 16781312 | tf_op jit(solution)/shard_map/dot_general | solution.py:37
  190.0 0.0 reduce-scatter.2.cloned.1.call-update
  190.0 88.8 %reduce-scatter.2.cloned.1.call-done = bf16[256,1024]{0,1:T(8,128)(2,1)} async-done(((bf16[2048,1024]{0,1:T(8,128)(2,1)}), bf16[256,1024]{0,1:T(8,128)(2,1)}) %reduce-scatter.2.cloned.1.call-update) | async-done | bytes 524304 | tf_op jit(solution)/shard_map/reduce_scatter | solution.py:36
  278.8 2.0 copy.17
  280.9 4.8 %copy.19 = bf16[1024,2048]{1,0:T(8,128)(2,1)} copy(bf16[1024,2048]{1,0:T(8,128)(2,1)} %all-gather.7.cloned.1.call-done) | data formatting | bytes 8388608
  (1 shorter events, 0.0 us)
Async XLA Ops:
  7.2 95.7 %all-gather.5.cloned.1.call-start = ((), (), s32[]{:S(2)}) async-start(), calls=%async_computation.3 | async-start | bytes 4718592 | tf_op jit(solution)/shard_map/all_gather | solution.py:29
  7.9 130.9 %all-gather.9.cloned.1.call-start = ((), (), s32[]{:S(2)}) async-start(), calls=%async_computation.6 | async-start | bytes 5242880 | tf_op jit(solution)/shard_map/all_gather | solution.py:24
  29.9 53.8 %copy-start = (f32[1024,512]{1,0:T(8,128)S(1)}, f32[1024,512]{1,0:T(8,128)}, u32[]{:S(2)}) copy-start(f32[1024,512]{1,0:T(8,128)} %param.7) | copy-start | bytes 6291460
  83.6 91.8 %all-gather.7.cloned.1.call-start = ((), (), s32[]{:S(2)}) async-start(), calls=%async_computation.4 | async-start | bytes 5242880 | tf_op jit(solution)/shard_map/all_gather | solution.py:25
  84.8 194.0 %reduce-scatter.2.cloned.1.call-start = ((), (), s32[]{:S(2)}) async-start(), calls=%async_computation.5 | async-start | bytes 4718592 | tf_op jit(solution)/shard_map/reduce_scatter | solution.py:36
Sparse Core Ops, SparseCore 0:
  10.0 92.7 all-gather.4
  104.4 34.3 all-gather.8
  141.0 34.4 all-gather.6
  190.1 88.6 reduce-scatter.1
where the time goes:
time: 293 us; the launch traced here: 292 us
  waiting for transfers between devices  172 us (59%)
  blocking collectives  72.2 us (25%)
  matrix products  14.5 us (5%)
  between operations  13.8 us (5%)
  local copies, waits for them, and re-layouts  13.4 us (5%)
  other arithmetic  5.95 us (2%)
    reduce_scatter x1, waiting for transfers between devices, shards(): lax.psum_scatter(lax.dot_general(down_full, hidden, (((0,), (1,)), ((), (...  88.8 us
    all_to_all x1, blocking collectives, shards(): lax.all_to_all(by_unit, 'fs', split_axis=2, concat_axis=0, tiled=True)  53.7 us
    all_gather x1, waiting for transfers between devices, shards(): lax.all_gather(arranged, ('gr', 'tp'), axis=1, tiled=True)  32.9 us
    all_gather x1, waiting for transfers between devices, shards(): lax.all_gather(down_cast, ('gr', 'tp'), axis=1, tiled=True)  31.7 us
    all_to_all x1, blocking collectives, shards(): lax.all_to_all(row_groups, ('gr', 'tp'), split_axis=0, concat_axis=2, til...  18.5 us
    all_gather x1, waiting for transfers between devices, shards(): piece = lax.all_gather(tokens, 'fs', axis=1, tiled=True)  18 us
    dot_general x1, matrix products, shards(): lax.dot_general(down_full, hidden, (((0,), (1,)), ((), ())), preferred_el...  14.5 us
    unnamed x4, local copies, waits for them, and re-layouts  6.83 us
  transfers between devices with their start and end apart: 4, of which 4 were waited for; matrix products, arithmetic and copies ran while one was open for 4% of the time, Pallas kernels for 0%

commit v1 on v0

--- a/solution.py
+++ b/solution.py
@@ -22,7 +22,12 @@
     arranged = by_owner.reshape(fs_count, 1, sub_rows, unit_width)
     stacked, down_full = (
         lax.all_gather(arranged, ("gr", "tp"), axis=1, tiled=True),
-        lax.all_gather(down_cast, ("gr", "tp"), axis=1, tiled=True),
+        jnp.concatenate(
+            lax.all_to_all(
+                jnp.stack([down_cast] * lax.axis_size(("gr", "tp"))), ("gr", "tp"), 0, 0
+            ),
+            axis=1,
+        ),
     )
     up_full = stacked.reshape(fs_count * group_count * sub_rows, unit_width)
     model_width = up_full.shape[0]

time: 293 us -> 280 us (0.956)
  waiting for transfers between devices: 172 us -> 79.4 us
  blocking collectives: 72.2 us -> 145 us
  local copies, waits for them, and re-layouts: 13.4 us -> 21.7 us
    all_to_all x0 -> x1, blocking collectives: none -> 73.1 us  [shards(): lax.all_to_all(jnp.stack([down_cast] * lax.axis_size(('gr', 'tp'))), ('gr...]
    all_gather x1, waiting for transfers between devices: 32.9 us -> 0.02 us  [shards(): lax.all_gather(arranged, ('gr', 'tp'), axis=1, tiled=True)]
    all_gather x1 -> x0, waiting for transfers between devices: 31.7 us -> none  [shards(): lax.all_gather(down_cast, ('gr', 'tp'), axis=1, tiled=True)]
    all_gather x1, waiting for transfers between devices: 18 us -> 0.01 us  [shards(): piece = lax.all_gather(tokens, 'fs', axis=1, tiled=True)]
    reduce_scatter x1, waiting for transfers between devices: 88.8 us -> 78.7 us  [shards(): lax.psum_scatter(lax.dot_general(down_full, hidden, (((0,), (1,)), ((), (...]
    all_to_all x0 -> x1, local copies, waits for them, and re-layouts: none -> 6.33 us  [shards(): lax.all_to_all(jnp.stack([down_cast] * lax.axis_size(('gr', 'tp'))), ('gr...]
  transfers between devices with their start and end apart: 4 -> 3, of which waited for: 4 -> 1; matrix products, arithmetic and copies ran while one was open for 4% -> 7% of each run, Pallas kernels for 0% -> 0%
where the time goes in v1:
time: 280 us
  blocking collectives  145 us (52%)
  waiting for transfers between devices  79.4 us (28%)
  local copies, waits for them, and re-layouts  21.7 us (8%)
  matrix products  14.5 us (5%)
  between operations  13.8 us (5%)
  other arithmetic  4.98 us (2%)
    reduce_scatter x1, waiting for transfers between devices, shards(): lax.psum_scatter(lax.dot_general(down_full, hidden, (((0,), (1,)), ((), (...  78.7 us
    all_to_all x1, blocking collectives, shards(): lax.all_to_all(jnp.stack([down_cast] * lax.axis_size(('gr', 'tp'))), ('gr...  73.1 us
    all_to_all x1, blocking collectives, shards(): lax.all_to_all(by_unit, 'fs', split_axis=2, concat_axis=0, tiled=True)  53.7 us
    all_to_all x1, blocking collectives, shards(): lax.all_to_all(row_groups, ('gr', 'tp'), split_axis=0, concat_axis=2, til...  18.5 us
    dot_general x1, matrix products, shards(): lax.dot_general(down_full, hidden, (((0,), (1,)), ((), ())), preferred_el...  14.5 us
    unnamed x4, local copies, waits for them, and re-layouts  8.48 us
    all_to_all x1, local copies, waits for them, and re-layouts, shards(): lax.all_to_all(jnp.stack([down_cast] * lax.axis_size(('gr', 'tp'))), ('gr...  6.33 us
  transfers between devices with their start and end apart: 3, of which 1 were waited for; matrix products, arithmetic and copies ran while one was open for 7% of the time, Pallas kernels for 0%

profile of v1, /device:TPU:0, one launch (start us, length us, event | category | flops | bytes accessed | tf_op | source)
XLA Modules:
  0.0 279.8 jit_solution(8483847400617460806)
XLA Ops:
  7.2 0.0 all-gather.4.cloned.1.call-start
  7.2 0.7 all-gather.4.cloned.1.call-update
  7.9 0.0 all-gather.6.cloned.1.call-start
  7.9 1.8 multiply_convert_fusion.1
  9.7 18.5 %all_to_all.35 = bf16[4,64,2048]{2,1,0:T(8,128)(2,1)S(1)} all-to-all(bf16[4,64,2048]{2,1,0:T(8,128)(2,1)S(1)} %bitcast.24), channel_id=1, replica_groups=mesh['gr'=2,'fs'=8,'tp'=2] {'gr','tp'}, dimensions={0} | all-to-all | bytes 2097152 | tf_op jit(solution)/shard_map/all_to_all | solution.py:17
  28.2 0.8 copy.18
  29.0 0.3 reshape.35
  29.3 0.6 copy.19
  29.9 0.0 copy-start
  29.9 53.7 %all_to_all.36 = bf16[1,64,8,1024]{3,1,0,2:T(8,128)(2,1)} all-to-all(bf16[1,64,8,1024]{3,1,0,2:T(8,128)(2,1)S(1)} %copy.19), channel_id=1, replica_groups=mesh['gr'=2,'fs'=8,'tp'=2] {'fs'}, dimensions={2} | all-to-all | bytes 2097152 | tf_op jit(solution)/shard_map/all_to_all | solution.py:21
  83.6 0.0 all-gather.6.cloned.1.call-update
  83.6 0.0 reduce-scatter.2.cloned.1.call-start
  83.7 0.0 copy-done
  83.7 0.1 convert_element_type.22
  83.8 0.3 stack.2
  84.2 73.1 %all_to_all.37 = bf16[4,1024,512]{2,1,0:T(8,128)(2,1)} all-to-all(bf16[4,1024,512]{2,1,0:T(8,128)(2,1)S(1)} %stack.2), channel_id=1, replica_groups=mesh['gr'=2,'fs'=8,'tp'=2] {'gr','tp'}, dimensions={0} | all-to-all | bytes 8388608 | tf_op jit(solution)/shard_map/all_to_all | solution.py:26
  157.2 6.3 %copy.22 = bf16[4,1024,512]{1,2,0:T(8,128)(2,1)} copy(bf16[4,1024,512]{2,1,0:T(8,128)(2,1)} %all_to_all.37) | data formatting | bytes 8388608 | tf_op jit(solution)/shard_map/all_to_all | solution.py:26
  163.6 0.0 all-gather.4.cloned.1.call-done
  163.6 3.1 %multiply_reduce_fusion = f32[1024]{0:T(1024)S(1)} fusion(bf16[1024,2048]{1,0:T(8,128)(2,1)} %all-gather.4.cloned.1.call-done), kind=kLoop, calls=%fused_computation | loop fusion | flops 6290432 | bytes 4198400 | tf_op jit(solution)/shard_map/reduce_sum | solution.py:37
  166.6 0.0 all-gather.6.cloned.1.call-done
  166.7 4.9 %copy.21 = bf16[8,4,64,1,1024]{4,2,1,0,3:T(8,128)(2,1)} copy(bf16[8,4,64,1,1024]{4,2,3,0,1:T(8,128)(2,1)} %all-gather.6.cloned.1.call-done) | data formatting | bytes 8388608 | tf_op jit(solution)/shard_map/all_gather | solution.py:24
  171.6 14.5 %convert_bitcast_fusion = bf16[2048,1024]{0,1:T(8,128)(2,1)} fusion(bf16[1024,2048]{0,1:T(8,128)(2,1)} %bitcast.18, bf16[2048,1024]{1,0:T(8,128)(2,1)} %bitcast.20, bf16[1024,2048]{1,0:T(8,128)(2,1)} %all-gather.4.cloned.1.call-done, f32[1024]{0:T(1024)S(1)} %add_rsqrt_fusion), kind=kOutput, calls=%fused_computation.1 | convolution fusion | flops 8596226048 | bytes 16781312 | tf_op jit(solution)/shard_map/dot_general | solution.py:42
  186.1 0.0 reduce-scatter.2.cloned.1.call-update
  186.1 6.4 %copy.24 = bf16[1024,2048]{1,0:T(8,128)(2,1)} copy(bf16[1024,2048]{0,1:T(8,128)(2,1)} %bitcast.19) | data formatting | bytes 8388608
  192.5 78.7 %reduce-scatter.2.cloned.1.call-done = bf16[256,1024]{0,1:T(8,128)(2,1)} async-done(((bf16[2048,1024]{0,1:T(8,128)(2,1)}), bf16[256,1024]{0,1:T(8,128)(2,1)}) %reduce-scatter.2.cloned.1.call-update) | async-done | bytes 524304 | tf_op jit(solution)/shard_map/reduce_scatter | solution.py:41
  271.2 2.0 copy.23
  (1 shorter events, 0.0 us)
Async XLA Ops:
  7.2 156.4 %all-gather.4.cloned.1.call-start = ((), (), s32[]{:S(2)}) async-start(), calls=%async_computation.4 | async-start | bytes 4718592 | tf_op jit(solution)/shard_map/all_gather | solution.py:34
  7.9 158.8 %all-gather.6.cloned.1.call-start = ((), (), s32[]{:S(2)}) async-start(), calls=%async_computation.6 | async-start | bytes 5242880 | tf_op jit(solution)/shard_map/all_gather | solution.py:24
  29.9 53.8 %copy-start = (f32[1024,512]{1,0:T(8,128)S(1)}, f32[1024,512]{1,0:T(8,128)}, u32[]{:S(2)}) copy-start(f32[1024,512]{1,0:T(8,128)} %param.7) | copy-start | bytes 6291460
  83.6 187.6 %reduce-scatter.2.cloned.1.call-start = ((), (), s32[]{:S(2)}) async-start(), calls=%async_computation.5 | async-start | bytes 4718592 | tf_op jit(solution)/shard_map/reduce_scatter | solution.py:41
Sparse Core Ops, SparseCore 0:
  10.0 92.7 all-gather.3
  104.4 55.3 all-gather.5
  186.2 84.9 reduce-scatter.1
